TPU v7x, 32 devices: a whole 2x2x4 slice. The times are simulated.
32 devices in a mesh: rep: 2 (over x), fs: 4 (over z), tp: 4 (over y, core).
Axes of the slice: x: 2, y: 2, z: 4, core: 2. Of those that a mesh axis runs over, the one named last changes fastest.
Arguments:
- tokens: bfloat16 [8192, 2048], P(('rep', 'fs'), 'tp'), may hold values from -6 to 6
- mix_in_gain: bfloat16 [2048], replicated, may hold values from 0.099609375 to 1.8984375
- bgate_weight: bfloat16 [2048, 2048], P('fs', 'tp'), may hold values from -0.125 to 0.125
- cgate_weight: bfloat16 [2048, 2048], P('fs', 'tp'), may hold values from -0.125 to 0.125
- value_weight: bfloat16 [2048, 2048], P('fs', 'tp'), may hold values from -0.125 to 0.125
- conv_taps: bfloat16 [3, 2048], replicated, may hold values from -3 to 3
- out_weight: bfloat16 [2048, 2048], P('tp', 'fs'), may hold values from -0.41984465 to 0.41984465
- mix_out_gain: bfloat16 [2048], replicated, may hold values from 0.099609375 to 1.8984375
- ffn_in_gain: bfloat16 [2048], replicated, may hold values from 0.099609375 to 1.8984375
- up_weight: bfloat16 [2048, 8192], P('fs', 'tp'), may hold values from -0.125 to 0.125
- down_weight: bfloat16 [8192, 2048], P('tp', 'fs'), may hold values from -0.20992233 to 0.20992233
- ffn_out_gain: bfloat16 [2048], replicated, may hold values from 0.099609375 to 1.8984375
Outputs:
- result: bfloat16 [8192, 2048], P(('rep', 'fs'), 'tp')
All inputs are finite; a program needn't handle non-finite values.
Results may differ from a plain program's by a relative error of at most 0.02.
Values may be sent and summed in bfloat16 or wider, within the bound.
A program may use at most 128 MiB of HBM per device.

v0:
```python
import jax
import jax.numpy as jnp
from jax import lax
from jax.sharding import PartitionSpec as P

LEN = 256
epsilon = 1e-06


def normalize(rows, gain):
    rows = rows.astype(jnp.float32)
    factor = lax.rsqrt(jnp.mean(rows * rows, axis=-1, keepdims=True) + epsilon)
    return rows * factor * gain.astype(jnp.float32)


def convolve(inner, taps):
    seqs = inner.reshape(-1, LEN, inner.shape[1])
    padded = jnp.pad(seqs, ((0, 0), (1, 1), (0, 0)))
    weights = taps.astype(jnp.float32)
    out = weights[0] * padded[:, :-2] + weights[1] * padded[:, 1:-1] + weights[2] * padded[:, 2:]
    return out.reshape(inner.shape)


def body(
    tokens,
    mix_in_gain,
    bgate_weight,
    cgate_weight,
    value_weight,
    conv_taps,
    out_weight,
    mix_out_gain,
    ffn_in_gain,
    up_weight,
    down_weight,
    ffn_out_gain,
):
    column = lax.axis_index("tp")
    own_width = tokens.shape[1]
    first = column * own_width
    full_width = mix_in_gain.shape[0]
    whole = lax.all_gather(tokens, "tp", axis=1, tiled=True)
    normed = normalize(whole, mix_in_gain).astype(jnp.bfloat16)

    def add_rows(piece):
        return jnp.dot(normed, piece, preferred_element_type=jnp.float32)

    bgate = add_rows(lax.all_gather(bgate_weight, "fs", axis=0, tiled=True))
    cgate = add_rows(lax.all_gather(cgate_weight, "fs", axis=0, tiled=True))
    value = add_rows(lax.all_gather(value_weight, "fs", axis=0, tiled=True))
    bgate = bgate.astype(jnp.bfloat16)
    cgate = cgate.astype(jnp.bfloat16)
    value = value.astype(jnp.bfloat16)
    channels = bgate.shape[1]
    own_taps = lax.dynamic_slice_in_dim(conv_taps, column * channels, channels, 1)
    inner = cgate.astype(jnp.float32) * value.astype(jnp.float32)
    gated = (bgate.astype(jnp.float32) * convolve(inner, own_taps)).astype(jnp.bfloat16)
    partial_mix = jnp.dot(
        gated,
        lax.all_gather(out_weight, "fs", axis=1, tiled=True),
        preferred_element_type=jnp.float32,
    )
    mixed = lax.psum(partial_mix.astype(jnp.bfloat16), "tp").astype(jnp.float32)
    resid = (whole.astype(jnp.float32) + normalize(mixed, mix_out_gain)).astype(jnp.bfloat16)
    resid_own = lax.dynamic_slice_in_dim(resid, first, own_width, 1)
    second = normalize(resid, ffn_in_gain).astype(jnp.bfloat16)
    lifted = jnp.dot(
        second,
        lax.all_gather(up_weight, "fs", axis=0, tiled=True),
        preferred_element_type=jnp.float32,
    )
    active = jnp.square(jnp.maximum(lifted, 0.0)).astype(jnp.bfloat16)
    partial_ffn = jnp.dot(
        active,
        lax.all_gather(down_weight, "fs", axis=1, tiled=True),
        preferred_element_type=jnp.float32,
    )
    ffn = lax.psum_scatter(
        partial_ffn.astype(jnp.bfloat16), "tp", scatter_dimension=1, tiled=True
    ).astype(jnp.float32)
    ffn_energy = lax.psum(jnp.sum(ffn * ffn, axis=1), "tp")
    out_gain = lax.dynamic_slice_in_dim(ffn_out_gain, first, own_width, 0).astype(jnp.float32)
    closing = ffn * lax.rsqrt(ffn_energy[:, None] / full_width + epsilon) * out_gain
    return (resid_own.astype(jnp.float32) + closing).astype(jnp.bfloat16)


def solution(mesh):
    placed = (
        P(("rep", "fs"), "tp"),
        P(),
        P("fs", "tp"),
        P("fs", "tp"),
        P("fs", "tp"),
        P(),
        P("tp", "fs"),
        P(),
        P(),
        P("fs", "tp"),
        P("tp", "fs"),
        P(),
    )
    return jax.shard_map(
        body, mesh=mesh, in_specs=placed, out_specs=P(("rep", "fs"), "tp"), check_vma=False
    )
```

profile of v0, /device:TPU:0, one launch (start us, length us, event | category | flops | bytes accessed | tf_op | source)
XLA Modules:
  0.0 707.6 jit_solution(8818610116150277627)
XLA Ops:
  6.5 0.0 all-gather.8.cloned.1.call-start
  6.5 0.7 all-gather.8.cloned.1.call-update
  7.3 0.0 all-gather.12.cloned.1.call-start
  7.3 0.7 all-gather.12.cloned.1.call-update
  8.0 0.0 all-gather.14.cloned.1.call-start
  8.1 0.7 all-gather.14.cloned.1.call-update
  8.7 0.0 all-gather.10.cloned.1.call-start
  8.8 0.5 all-gather.10.cloned.1.call-update
  9.3 0.0 all-gather.16.cloned.1.call-start
  9.4 0.5 all-gather.16.cloned.1.call-update
  9.9 0.0 all-reduce.3.cloned.1.call-start
  10.0 0.7 dynamic-slice_convert_fusion
  10.7 0.7 convert_element_type.76
  11.4 34.8 %all-gather.8.cloned.1.call-done = bf16[1024,2048]{1,0:T(8,128)(2,1)} async-done(((bf16[1024,512]{1,0:T(8,128)(2,1)}), bf16[1024,2048]{1,0:T(8,128)(2,1)}) %all-gather.8.cloned.1.call-update) | async-done | bytes 4194320 | tf_op jit(solution)/shard_map/all_gather | solution.py:42
  46.1 3.1 fusion.5
  49.2 44.2 %all-gather.12.cloned.1.call-done = bf16[2048,512]{1,0:T(8,128)(2,1)} async-done(((bf16[512,512]{1,0:T(8,128)(2,1)}), bf16[2048,512]{1,0:T(8,128)(2,1)}) %all-gather.12.cloned.1.call-update) | async-done | bytes 2097168 | tf_op jit(solution)/shard_map/all_gather | solution.py:49
  93.4 5.2 convolution_convert_fusion.2
  98.6 40.8 %all-gather.14.cloned.1.call-done = bf16[2048,512]{1,0:T(8,128)(2,1)} async-done(((bf16[512,512]{1,0:T(8,128)(2,1)}), bf16[2048,512]{1,0:T(8,128)(2,1)}) %all-gather.14.cloned.1.call-update) | async-done | bytes 2097168 | tf_op jit(solution)/shard_map/all_gather | solution.py:50
  139.4 5.2 convert_multiply_fusion.8
  144.7 0.6 multiply_add_fusion
  145.3 40.0 %all-gather.10.cloned.1.call-done = bf16[2048,512]{1,0:T(8,128)(2,1)} async-done(((bf16[512,512]{1,0:T(8,128)(2,1)}), bf16[2048,512]{1,0:T(8,128)(2,1)}) %all-gather.10.cloned.1.call-update) | async-done | bytes 2097168 | tf_op jit(solution)/shard_map/all_gather | solution.py:48
  185.4 5.2 fusion.25
  190.6 40.7 %all-gather.16.cloned.1.call-done = bf16[512,2048]{1,0:T(8,128)(2,1)} async-done(((bf16[512,512]{1,0:T(8,128)(2,1)}), bf16[512,2048]{1,0:T(8,128)(2,1)}) %all-gather.16.cloned.1.call-update) | async-done | bytes 2097168 | tf_op jit(solution)/shard_map/all_gather | solution.py:60
  231.3 5.9 convolution_convert_fusion
  237.2 0.0 copy-start.1
  237.2 0.0 copy-start.2
  237.2 0.0 all-reduce.3.cloned.1.call-update
  237.2 0.0 all-gather.18.cloned.1.call-start
  237.2 0.7 all-gather.18.cloned.1.call-update
  237.9 0.0 all-gather.20.cloned.1.call-start
  238.0 0.7 all-gather.20.cloned.1.call-update
  238.7 0.2 reduce-scatter.2.cloned.1.call-start
  238.9 0.0 copy-done.1
  238.9 0.0 copy-done.2
  239.0 82.7 %all-reduce.3.cloned.1.call-done = bf16[1024,2048]{1,0:T(8,128)(2,1)} async-done(((bf16[1024,2048]{1,0:T(8,128)(2,1)}), bf16[1024,2048]{1,0:T(8,128)(2,1)}) %all-reduce.3.cloned.1.call-update) | async-done | bytes 4194320 | tf_op jit(solution)/shard_map/psum | solution.py:63
  321.6 0.0 copy-start
  321.6 3.2 fusion
  324.9 0.2 copy-done
  325.1 5.3 fusion.2
  330.4 142.6 %all-gather.18.cloned.1.call-done = bf16[2048,2048]{1,0:T(8,128)(2,1)} async-done(((bf16[512,2048]{1,0:T(8,128)(2,1)}), bf16[2048,2048]{1,0:T(8,128)(2,1)}) %all-gather.18.cloned.1.call-update) | async-done | bytes 8388624 | tf_op jit(solution)/shard_map/all_gather | solution.py:69
  473.0 149.4 %all-gather.20.cloned.1.call-done = bf16[2048,2048]{1,0:T(8,128)(2,1)} async-done(((bf16[2048,512]{1,0:T(8,128)(2,1)}), bf16[2048,2048]{1,0:T(8,128)(2,1)}) %all-gather.20.cloned.1.call-update) | async-done | bytes 8388624 | tf_op jit(solution)/shard_map/all_gather | solution.py:75
  622.4 25.7 %fusion.18 = bf16[1024,2048]{1,0:T(8,128)(2,1)} fusion(bf16[2048,2048]{1,0:T(8,128)(2,1)} %all-gather.20.cloned.1.call-done, bf16[2048,2048]{1,0:T(8,128)(2,1)} %all-gather.18.cloned.1.call-done, bf16[1024,2048]{1,0:T(8,128)(2,1)} %get-tuple-element.6, f32[2048]{0:T(1024)S(1)} %convert_element_type.92, f32[1024]{0:T(1024)S(1)} %add_rsqrt_fusion.1), kind=kOutput, calls=%fused_computation.22 | convolution fusion | flops 17196646400 | bytes 25178112 | tf_op jit(solution)/shard_map/dot_general | solution.py:73
  648.1 0.0 reduce-scatter.2.cloned.1.call-update
  648.1 0.8 dynamic-slice_convert_fusion.1
  648.8 41.9 %reduce-scatter.2.cloned.1.call-done = bf16[1024,512]{1,0:T(8,128)(2,1)} async-done(((bf16[1024,2048]{1,0:T(8,128)(2,1)}), bf16[1024,512]{1,0:T(8,128)(2,1)}) %reduce-scatter.2.cloned.1.call-update) | async-done | bytes 1048592 | tf_op jit(solution)/shard_map/reduce_scatter | solution.py:78
  690.8 1.5 fusion.21
  692.3 5.8 psum.15
  698.1 3.0 fusion.24
  (7 shorter events, 0.0 us)
Async XLA Ops:
  6.5 39.6 %all-gather.8.cloned.1.call-start = ((), (), s32[]{:S(2)}) async-start(), calls=%async_computation.1 | async-start | bytes 5242880 | tf_op jit(solution)/shard_map/all_gather | solution.py:42
  7.3 86.1 %all-gather.12.cloned.1.call-start = ((), (), s32[]{:S(2)}) async-start(), calls=%async_computation.3 | async-start | bytes 2621440 | tf_op jit(solution)/shard_map/all_gather | solution.py:49
  8.0 131.4 %all-gather.14.cloned.1.call-start = ((), (), s32[]{:S(2)}) async-start(), calls=%async_computation.4 | async-start | bytes 2621440 | tf_op jit(solution)/shard_map/all_gather | solution.py:50
  8.7 176.6 %all-gather.10.cloned.1.call-start = ((), (), s32[]{:S(2)}) async-start(), calls=%async_computation.2 | async-start | bytes 2621440 | tf_op jit(solution)/shard_map/all_gather | solution.py:48
  9.3 221.9 %all-gather.16.cloned.1.call-start = ((), (), s32[]{:S(2)}) async-start(), calls=%async_computation.5 | async-start | bytes 2621440 | tf_op jit(solution)/shard_map/all_gather | solution.py:60
  9.9 311.7 %all-reduce.3.cloned.1.call-start = ((), (), s32[]{:S(2)}) async-start(), calls=%async_computation.6 | async-start | bytes 8388608 | tf_op jit(solution)/shard_map/psum | solution.py:63
  237.2 1.8 copy-start.1
  237.2 1.8 copy-start.2
  237.2 235.8 %all-gather.18.cloned.1.call-start = ((), (), s32[]{:S(2)}) async-start(), calls=%async_computation.7 | async-start | bytes 10485760 | tf_op jit(solution)/shard_map/all_gather | solution.py:69
  237.9 384.4 %all-gather.20.cloned.1.call-start = ((), (), s32[]{:S(2)}) async-start(), calls=%async_computation.8 | async-start | bytes 10485760 | tf_op jit(solution)/shard_map/all_gather | solution.py:75
  238.7 452.1 %reduce-scatter.2.cloned.1.call-start = ((), (), s32[]{:S(2)}) async-start(), calls=%async_computation.9 | async-start | bytes 5242880 | tf_op jit(solution)/shard_map/reduce_scatter | solution.py:78
  321.6 3.4 copy-start
Sparse Core Ops, SparseCore 0:
  8.9 37.1 all-gather.7
  47.7 45.6 all-gather.11
  94.9 44.4 all-gather.13
  140.9 44.4 all-gather.9
  186.8 44.4 all-gather.15
  237.3 84.2 all-reduce.2
  323.2 149.7 all-gather.17
  474.6 147.7 all-gather.19
  648.2 42.5 reduce-scatter.1
where the time goes:
time: 708 us
  waiting for transfers between devices  622 us (88%)
  matrix products  47.3 us (7%)
  other arithmetic  18.9 us (3%)
  between operations  13.3 us (2%)
    all_gather x1, waiting for transfers between devices, body(): lax.all_gather(down_weight, 'fs', axis=1, tiled=True)  149 us
    all_gather x1, waiting for transfers between devices, body(): lax.all_gather(up_weight, 'fs', axis=0, tiled=True)  143 us
    psum x1, waiting for transfers between devices, body(): mixed = lax.psum(partial_mix.astype(jnp.bfloat16), 'tp').astype(jnp.float32)  82.7 us
    all_gather x1, waiting for transfers between devices, body(): cgate = add_rows(lax.all_gather(cgate_weight, 'fs', axis=0, tiled=True))  44.2 us
    reduce_scatter x1, waiting for transfers between devices, body(): lax.psum_scatter(partial_ffn.astype(jnp.bfloat16), 'tp', scatter_dimensio...  41.9 us
    all_gather x1, waiting for transfers between devices, body(): value = add_rows(lax.all_gather(value_weight, 'fs', axis=0, tiled=True))  40.8 us
    all_gather x1, waiting for transfers between devices, body(): lax.all_gather(out_weight, 'fs', axis=1, tiled=True)  40.7 us
    all_gather x1, waiting for transfers between devices, body(): bgate = add_rows(lax.all_gather(bgate_weight, 'fs', axis=0, tiled=True))  40 us
  transfers between devices with their start and end apart: 9, of which 9 were waited for; matrix products, arithmetic and copies ran while one was open for 4% of the time, Pallas kernels for 0%

commit v1 on v0

--- a/solution.py
+++ b/solution.py
@@ -5,6 +5,12 @@
 
 LEN = 256
 epsilon = 1e-06
+
+
+def all_parts(block, axis, d):
+    parts = lax.all_gather(block, axis, axis=0, tiled=False)
+    whole = jnp.concatenate(parts, axis=d)
+    return whole
 
 
 def normalize(rows, gain):
@@ -71,9 +77,7 @@
     )
     active = jnp.square(jnp.maximum(lifted, 0.0)).astype(jnp.bfloat16)
     partial_ffn = jnp.dot(
-        active,
-        lax.all_gather(down_weight, "fs", axis=1, tiled=True),
-        preferred_element_type=jnp.float32,
+        active, all_parts(down_weight, "fs", 1), preferred_element_type=jnp.float32
     )
     ffn = lax.psum_scatter(
         partial_ffn.astype(jnp.bfloat16), "tp", scatter_dimension=1, tiled=True

time: 708 us -> 708 us (level)
  waiting for transfers between devices: 622 us -> 610 us
  local copies, waits for them, and re-layouts: 0.23 us -> 12 us
    reshape x0 -> x1, local copies, waits for them, and re-layouts: none -> 11.8 us  [all_parts(): whole = jnp.concatenate(parts, axis=d)]
  transfers between devices with their start and end apart: 9 -> 9, of which waited for: 9 -> 9; matrix products, arithmetic and copies ran while one was open for 4% -> 6% of each run, Pallas kernels for 0% -> 0%
where the time goes in v1:
time: 708 us
  waiting for transfers between devices  610 us (86%)
  matrix products  47.3 us (7%)
  other arithmetic  18.9 us (3%)
  between operations  13.3 us (2%)
  local copies, waits for them, and re-layouts  12 us (2%)
    all_gather x1, waiting for transfers between devices, all_parts(): parts = lax.all_gather(block, axis, axis=0, tiled=False)  143 us
    all_gather x1, waiting for transfers between devices, body(): lax.all_gather(up_weight, 'fs', axis=0, tiled=True)  138 us
    psum x1, waiting for transfers between devices, body(): mixed = lax.psum(partial_mix.astype(jnp.bfloat16), 'tp').astype(jnp.float32)  82.7 us
    all_gather x1, waiting for transfers between devices, body(): cgate = add_rows(lax.all_gather(cgate_weight, 'fs', axis=0, tiled=True))  44.2 us
    reduce_scatter x1, waiting for transfers between devices, body(): lax.psum_scatter(partial_ffn.astype(jnp.bfloat16), 'tp', scatter_dimensio...  42 us
    all_gather x1, waiting for transfers between devices, body(): value = add_rows(lax.all_gather(value_weight, 'fs', axis=0, tiled=True))  40.8 us
    all_gather x1, waiting for transfers between devices, body(): lax.all_gather(out_weight, 'fs', axis=1, tiled=True)  40.7 us
    all_gather x1, waiting for transfers between devices, body(): bgate = add_rows(lax.all_gather(bgate_weight, 'fs', axis=0, tiled=True))  40 us
  transfers between devices with their start and end apart: 9, of which 9 were waited for; matrix products, arithmetic and copies ran while one was open for 6% of the time, Pallas kernels for 0%

profile of v1, /device:TPU:0, one launch (start us, length us, event | category | flops | bytes accessed | tf_op | source)
XLA Modules:
  0.0 707.6 jit_solution(8327947060965505404)
XLA Ops:
  6.5 0.0 all-gather.9.cloned.1.call-start
  6.5 0.7 all-gather.9.cloned.1.call-update
  7.3 0.0 all-gather.13.cloned.1.call-start
  7.3 0.7 all-gather.13.cloned.1.call-update
  8.0 0.0 all-gather.15.cloned.1.call-start
  8.1 0.7 all-gather.15.cloned.1.call-update
  8.7 0.0 all-gather.11.cloned.1.call-start
  8.8 0.5 all-gather.11.cloned.1.call-update
  9.3 0.0 all-gather.17.cloned.1.call-start
  9.4 0.5 all-gather.17.cloned.1.call-update
  9.9 0.0 all-reduce.3.cloned.1.call-start
  10.0 0.7 dynamic-slice_convert_fusion
  10.7 0.7 convert_element_type.76
  11.4 34.8 %all-gather.9.cloned.1.call-done = bf16[1024,2048]{1,0:T(8,128)(2,1)} async-done(((bf16[1024,512]{1,0:T(8,128)(2,1)}), bf16[1024,2048]{1,0:T(8,128)(2,1)}) %all-gather.9.cloned.1.call-update) | async-done | bytes 4194320 | tf_op jit(solution)/shard_map/all_gather | solution.py:48
  46.1 3.1 fusion.5
  49.2 44.2 %all-gather.13.cloned.1.call-done = bf16[2048,512]{1,0:T(8,128)(2,1)} async-done(((bf16[512,512]{1,0:T(8,128)(2,1)}), bf16[2048,512]{1,0:T(8,128)(2,1)}) %all-gather.13.cloned.1.call-update) | async-done | bytes 2097168 | tf_op jit(solution)/shard_map/all_gather | solution.py:55
  93.4 5.2 convolution_convert_fusion.2
  98.6 40.8 %all-gather.15.cloned.1.call-done = bf16[2048,512]{1,0:T(8,128)(2,1)} async-done(((bf16[512,512]{1,0:T(8,128)(2,1)}), bf16[2048,512]{1,0:T(8,128)(2,1)}) %all-gather.15.cloned.1.call-update) | async-done | bytes 2097168 | tf_op jit(solution)/shard_map/all_gather | solution.py:56
  139.4 5.2 convert_multiply_fusion.8
  144.7 0.6 multiply_add_fusion
  145.3 40.0 %all-gather.11.cloned.1.call-done = bf16[2048,512]{1,0:T(8,128)(2,1)} async-done(((bf16[512,512]{1,0:T(8,128)(2,1)}), bf16[2048,512]{1,0:T(8,128)(2,1)}) %all-gather.11.cloned.1.call-update) | async-done | bytes 2097168 | tf_op jit(solution)/shard_map/all_gather | solution.py:54
  185.4 5.2 fusion.25
  190.6 40.7 %all-gather.17.cloned.1.call-done = bf16[512,2048]{1,0:T(8,128)(2,1)} async-done(((bf16[512,512]{1,0:T(8,128)(2,1)}), bf16[512,2048]{1,0:T(8,128)(2,1)}) %all-gather.17.cloned.1.call-update) | async-done | bytes 2097168 | tf_op jit(solution)/shard_map/all_gather | solution.py:66
  231.3 5.9 convolution_convert_fusion
  237.2 0.0 copy-start.1
  237.2 0.0 copy-start.2
  237.2 0.0 all-reduce.3.cloned.1.call-update
  237.2 0.0 all-gather.21.cloned.1.call-start
  237.2 0.7 all-gather.21.cloned.1.call-update
  237.9 0.0 all-gather.19.cloned.1.call-start
  238.0 0.7 all-gather.19.cloned.1.call-update
  238.7 0.2 reduce-scatter.2.cloned.1.call-start
  238.9 0.0 copy-done.1
  238.9 0.0 copy-done.2
  239.0 82.7 %all-reduce.3.cloned.1.call-done = bf16[1024,2048]{1,0:T(8,128)(2,1)} async-done(((bf16[1024,2048]{1,0:T(8,128)(2,1)}), bf16[1024,2048]{1,0:T(8,128)(2,1)}) %all-reduce.3.cloned.1.call-update) | async-done | bytes 4194320 | tf_op jit(solution)/shard_map/psum | solution.py:69
  321.6 3.2 fusion
  324.9 0.2 copy-done
  325.1 5.3 fusion.2
  330.4 142.6 %all-gather.21.cloned.1.call-done = bf16[8192,512]{1,0:T(8,128)(2,1)} async-done(((bf16[2048,512]{1,0:T(8,128)(2,1)}), bf16[8192,512]{1,0:T(8,128)(2,1)}) %all-gather.21.cloned.1.call-update) | async-done | bytes 8388624 | tf_op jit(solution)/shard_map/all_gather | solution.py:11
  473.0 11.8 %copy.13 = bf16[2048,4,512]{0,2,1:T(8,128)(2,1)} copy(bf16[2048,4,512]{2,0,1:T(8,128)(2,1)} %bitcast.19) | data formatting | bytes 16777216 | tf_op jit(solution)/shard_map/reshape | solution.py:12
  484.8 137.6 %all-gather.19.cloned.1.call-done = bf16[2048,2048]{1,0:T(8,128)(2,1)} async-done(((bf16[512,2048]{1,0:T(8,128)(2,1)}), bf16[2048,2048]{1,0:T(8,128)(2,1)}) %all-gather.19.cloned.1.call-update) | async-done | bytes 8388624 | tf_op jit(solution)/shard_map/all_gather | solution.py:75
  622.4 25.6 %fusion.18 = bf16[1024,2048]{1,0:T(8,128)(2,1)} fusion(bf16[2048,2048]{0,1:T(8,128)(2,1)} %bitcast.20, bf16[2048,2048]{1,0:T(8,128)(2,1)} %all-gather.19.cloned.1.call-done, bf16[1024,2048]{1,0:T(8,128)(2,1)} %get-tuple-element.6, f32[2048]{0:T(1024)S(1)} %convert_element_type.92, f32[1024]{0:T(1024)S(1)} %add_rsqrt_fusion.1), kind=kOutput, calls=%fused_computation.22 | convolution fusion | flops 17196646400 | bytes 25178112 | tf_op jit(solution)/shard_map/dot_general | solution.py:79
  648.0 0.0 reduce-scatter.2.cloned.1.call-update
  648.0 0.8 dynamic-slice_convert_fusion.1
  648.8 42.0 %reduce-scatter.2.cloned.1.call-done = bf16[1024,512]{1,0:T(8,128)(2,1)} async-done(((bf16[1024,2048]{1,0:T(8,128)(2,1)}), bf16[1024,512]{1,0:T(8,128)(2,1)}) %reduce-scatter.2.cloned.1.call-update) | async-done | bytes 1048592 | tf_op jit(solution)/shard_map/reduce_scatter | solution.py:82
  690.8 1.5 fusion.21
  692.3 5.8 psum.15
  698.1 3.0 fusion.24
  (8 shorter events, 0.0 us)
Async XLA Ops:
  6.5 39.6 %all-gather.9.cloned.1.call-start = ((), (), s32[]{:S(2)}) async-start(), calls=%async_computation.1 | async-start | bytes 5242880 | tf_op jit(solution)/shard_map/all_gather | solution.py:48
  7.3 86.1 %all-gather.13.cloned.1.call-start = ((), (), s32[]{:S(2)}) async-start(), calls=%async_computation.3 | async-start | bytes 2621440 | tf_op jit(solution)/shard_map/all_gather | solution.py:55
  8.0 131.4 %all-gather.15.cloned.1.call-start = ((), (), s32[]{:S(2)}) async-start(), calls=%async_computation.4 | async-start | bytes 2621440 | tf_op jit(solution)/shard_map/all_gather | solution.py:56
  8.7 176.6 %all-gather.11.cloned.1.call-start = ((), (), s32[]{:S(2)}) async-start(), calls=%async_computation.2 | async-start | bytes 2621440 | tf_op jit(solution)/shard_map/all_gather | solution.py:54
  9.3 221.9 %all-gather.17.cloned.1.call-start = ((), (), s32[]{:S(2)}) async-start(), calls=%async_computation.5 | async-start | bytes 2621440 | tf_op jit(solution)/shard_map/all_gather | solution.py:66
  9.9 311.7 %all-reduce.3.cloned.1.call-start = ((), (), s32[]{:S(2)}) async-start(), calls=%async_computation.6 | async-start | bytes 8388608 | tf_op jit(solution)/shard_map/psum | solution.py:69
  237.2 1.8 copy-start.1
  237.2 1.8 copy-start.2
  237.2 235.8 %all-gather.21.cloned.1.call-start = ((), (), s32[]{:S(2)}) async-start(), calls=%async_computation.9 | async-start | bytes 10485760 | tf_op jit(solution)/shard_map/all_gather | solution.py:11
  237.9 384.4 %all-gather.19.cloned.1.call-start = ((), (), s32[]{:S(2)}) async-start(), calls=%async_computation.7 | async-start | bytes 10485760 | tf_op jit(solution)/shard_map/all_gather | solution.py:75
  238.7 452.1 %reduce-scatter.2.cloned.1.call-start = ((), (), s32[]{:S(2)}) async-start(), calls=%async_computation.8 | async-start | bytes 5242880 | tf_op jit(solution)/shard_map/reduce_scatter | solution.py:82
  321.6 3.4 copy-start
Sparse Core Ops, SparseCore 0:
  8.9 37.1 all-gather.8
  47.7 45.6 all-gather.12
  94.9 44.4 all-gather.14
  140.9 44.4 all-gather.10
  186.8 44.4 all-gather.16
  237.3 84.2 all-reduce.2
  323.2 149.7 all-gather.20
  474.6 147.7 all-gather.18
  648.1 42.6 reduce-scatter.1
